TPU v7x, 512 devices: a whole 4x8x8 slice. The times are simulated.
512 devices in a mesh: sp: 32 (over z, x), tp: 16 (over y, core).
Axes of the slice: x: 4, y: 8, z: 8, core: 2. Of those that a mesh axis runs over, the one named last changes fastest.
Arguments:
- outer_gate: bfloat16 [8192, 2048], P('sp', 'tp'), may hold values from -6 to 6
- inner_gate: bfloat16 [8192, 2048], P('sp', 'tp'), may hold values from -6 to 6
- conv_input: bfloat16 [8192, 2048], P('sp', 'tp'), may hold values from -6 to 6
- conv_weight: bfloat16 [3, 2048], P(None, 'tp'), may hold values from -3.5 to 3.5
- doc_ids: int32 [8192], P('sp'), may hold values from 0 to 15, as said below
- output_weight: bfloat16 [2048, 4096], P(None, 'tp'), may hold values from -0.125 to 0.125
- residual: bfloat16 [8192, 4096], P('sp', 'tp'), as said below
- norm_gain: bfloat16 [4096], P('tp'), may hold values from 0.099609375 to 1.8984375
- expert_ids: int32 [8192, 2], P('sp'), may hold values from 0 to 31, all different within a row; in each aligned block of 256 rows (0 to 255, 256 to 511, ...) at most 32 rows name the same one
- group_weight: float32 [8192], P('sp'), may hold values from 0.25 to 1
- expert_weight: float32 [8192, 2], P('sp'), may hold values from 0.05 to 1
- gate_weight: bfloat16 [32, 4096, 2048], P('sp', None, 'tp'), may hold values from -0.09375 to 0.09375
- up_weight: bfloat16 [32, 4096, 2048], P('sp', None, 'tp'), may hold values from -0.09375 to 0.09375
- down_weight: bfloat16 [32, 2048, 4096], P('sp', None, 'tp'), may hold values from -0.125 to 0.125
Outputs:
- layer_out: bfloat16 [8192, 4096], P('sp', 'tp')
Inputs may be any that keep to these rules, and one draw needn't show every extreme that they name: `expert_ids`: within the 256 rows of one index of sp no expert is named more than 32 times, a bound that some block reaches; the two experts of a row differ. `doc_ids`: never falling along positions, rising by one at each document's start; every document has 256 to 768 positions, and one exactly 768. `residual`: Columns' scales are of order one to ten.
All inputs are finite; a program needn't handle non-finite values.
Results may differ from a plain program's by a relative error of at most 0.009.
Values may be sent and summed in bfloat16 or wider, within the bound.
A program may use at most 64 MiB of HBM per device.

v0:
```python
import jax
import jax.numpy as jnp
from jax import lax
from jax.sharding import PartitionSpec as P

EPS = 1e-06


def passed_along(value, axis, steps):
    count = lax.axis_size(axis)
    initial, last = (max(0, -steps), min(count, count - steps))
    return lax.ppermute(value, axis, [(source, source + steps) for source in range(initial, last)])


def from_everyone(x, axis):
    copies = jnp.broadcast_to(x, (lax.axis_size(axis), *x.shape))
    return lax.all_to_all(copies, axis, split_axis=0, concat_axis=0, tiled=True)


def joined_along(blocks, dim):
    dims = list(blocks.shape[1:])
    dims[dim] *= blocks.shape[0]
    return jnp.moveaxis(blocks, 0, dim).reshape(dims)


def collect(x, axis, dim):
    blocks = from_everyone(x, axis)
    return joined_along(blocks, dim)


def of_everyone(x, axis):
    everything = from_everyone(x, axis)
    return jnp.sum(everything, axis=0)


def per_device(
    outer_gate,
    inner_gate,
    conv_input,
    conv_weight,
    doc_ids,
    output_weight,
    residual,
    norm_gain,
    expert_ids,
    group_weight,
    expert_weight,
    gate_weight,
    up_weight,
    down_weight,
):
    row_count = conv_input.shape[0]
    products = inner_gate.astype(jnp.float32) * conv_input.astype(jnp.float32)
    own_docs = doc_ids.astype(jnp.float32)
    tail_rows, tail_docs = passed_along((products[-2:], own_docs[-2:]), "sp", 1)
    ext_products = jnp.concatenate([tail_rows, products], axis=0)
    ext_docs = jnp.concatenate([tail_docs, own_docs], axis=0)
    taps = conv_weight.astype(jnp.float32)
    conv = taps[2] * products
    for shift_by in (1, 2):
        first = 2 - shift_by
        same_doc = (ext_docs[first : first + row_count] == own_docs)[:, None]
        conv = conv + jnp.where(
            same_doc, taps[2 - shift_by] * ext_products[first : first + row_count], 0.0
        )
    branch = (outer_gate.astype(jnp.float32) * conv).astype(jnp.bfloat16)
    cols_local = output_weight.shape[1]
    branch_sum = jnp.dot(
        collect(branch, "tp", 1), output_weight, preferred_element_type=jnp.float32
    )
    resid = (residual.astype(jnp.float32) + branch_sum).astype(jnp.bfloat16)
    resid_wide = resid.astype(jnp.float32)
    total_sq = of_everyone(jnp.sum(resid_wide * resid_wide, axis=1), "tp")
    width = cols_local * lax.axis_size("tp")
    scale = lax.rsqrt(total_sq / width + EPS)[:, None]
    normed = (resid_wide * scale * norm_gain.astype(jnp.float32)).astype(jnp.bfloat16)
    experts = lax.axis_size("sp")
    capacity = 4 * row_count // experts
    flat_experts = expert_ids.reshape(-1)
    onehot = (flat_experts[:, None] == jnp.arange(experts, dtype=jnp.int32)[None, :]).astype(
        jnp.int32
    )
    slot_rank = jnp.sum((jnp.cumsum(onehot, axis=0) - onehot) * onehot, axis=1)
    slot_index = flat_experts * capacity + slot_rank
    token_of = jnp.arange(2 * row_count, dtype=jnp.int32) // 2
    token_table = jnp.full((experts * capacity,), row_count, jnp.int32).at[slot_index].set(token_of)
    gate_local = gate_weight[0]
    up_local = up_weight[0]
    arrived_rows = experts * capacity
    padded = jnp.concatenate([normed, jnp.zeros((1, cols_local), jnp.bfloat16)], axis=0)
    outgoing = padded[token_table].reshape(experts, capacity, cols_local)
    arrived = lax.all_to_all(outgoing, "sp", split_axis=0, concat_axis=0, tiled=True).reshape(
        arrived_rows, cols_local
    )
    piece = lax.all_gather(arrived, "tp", axis=1, tiled=True)
    gate_val = jnp.dot(piece, gate_local, preferred_element_type=jnp.float32)
    up_val = jnp.dot(piece, up_local, preferred_element_type=jnp.float32)
    hidden = (jax.nn.silu(gate_val) * up_val).astype(jnp.bfloat16)
    down_local = down_weight[0]
    expert_out = jnp.dot(
        lax.all_gather(hidden, "tp", axis=1, tiled=True),
        down_local,
        preferred_element_type=jnp.float32,
    ).astype(jnp.bfloat16)
    returned = lax.all_to_all(
        expert_out.reshape(experts, capacity, cols_local),
        "sp",
        split_axis=0,
        concat_axis=0,
        tiled=True,
    )
    picked = (
        returned.reshape(arrived_rows, cols_local)[slot_index]
        .reshape(row_count, 2, cols_local)
        .astype(jnp.float32)
    )
    mix_weight = (
        group_weight[:, None] * expert_weight / jnp.sum(expert_weight, axis=1, keepdims=True)
    )
    routed_sum = jnp.sum(picked * mix_weight[:, :, None], axis=1)
    return (resid_wide + routed_sum).astype(jnp.bfloat16)


def solution(mesh):
    return jax.shard_map(
        per_device,
        mesh=mesh,
        in_specs=(
            P("sp", "tp"),
            P("sp", "tp"),
            P("sp", "tp"),
            P(None, "tp"),
            P("sp"),
            P(None, "tp"),
            P("sp", "tp"),
            P("tp"),
            P("sp", None),
            P("sp"),
            P("sp", None),
            P("sp", None, "tp"),
            P("sp", None, "tp"),
            P("sp", None, "tp"),
        ),
        out_specs=P("sp", "tp"),
        check_vma=False,
    )
```

profile of v0, /device:TPU:8, one launch (start us, length us, event | category | flops | bytes accessed | tf_op | source)
XLA Modules:
  0.0 263.7 jit_solution(17630297964401948509)
XLA Ops:
  6.5 0.0 copy-start
  6.5 0.0 copy-start.4
  6.5 0.8 convert_element_type.60
  7.4 0.1 slice.34
  7.4 3.4 %collective-permute-start = (f32[2]{0:T(128)S(1)}, f32[2]{0:T(128)S(1)}, u32[]{:S(2)}, u32[]{:S(2)}) collective-permute-start(f32[2]{0:T(128)S(1)} %slice.34), channel_id=1, source_target_pairs={{0,16},{16,32},{32,48},{48,64},{64,80},{80,96},{96,112},{112,128},... | collective-permute-start | bytes 32 | tf_op jit(solution)/shard_map/ppermute | solution.py:12
  10.8 0.9 convert_multiply_fusion
  11.7 3.4 %collective-permute-start.1 = (f32[2,128]{1,0:T(2,128)S(1)}, f32[2,128]{1,0:T(2,128)S(1)}, u32[]{:S(2)}, u32[]{:S(2)}) collective-permute-start(f32[2,128]{1,0:T(2,128)S(1)} %slice.48), channel_id=1, source_target_pairs={{0,16},{16,32},{32,48},{48,64},{64,80},{80,96},{96,112},{112,128},... | collective-permute-start | bytes 3080 | tf_op jit(solution)/shard_map/ppermute | solution.py:12
  15.1 0.7 convert_element_type.57
  15.8 0.0 collective-permute-done
  15.8 0.1 pad_maximum_fusion.1
  15.9 0.8 slice_compare_fusion.1
  16.7 0.0 collective-permute-done.1
  16.7 1.0 fusion.13
  17.7 0.1 copy.28
  17.8 1.1 broadcast_in_dim.44
  18.9 7.6 %all-to-all-start = ((bf16[16,256,128]{1,2,0:T(8,128)(2,1)}), bf16[16,256,128]{1,2,0:T(8,128)(2,1)S(1)}, u32[]{:S(2)}, u32[]{:S(2)}) async-start(bf16[16,256,128]{1,2,0:T(8,128)(2,1)} %broadcast_in_dim.44), calls=%async_computation | async-start | bytes 2097152 | tf_op jit(solution)/shard_map/all_to_all | solution.py:17
  26.4 0.8 copy.31
  27.2 0.1 eq.37
  27.4 0.1 eq.33
  27.5 1.2 reduce-window.6
  28.7 0.2 slice_reduce_fusion
  29.0 0.7 broadcast_multiply_fusion
  29.7 0.1 copy.30
  29.8 0.1 mul.115
  30.0 0.1 fusion.18
  30.1 2.4 scatter_custom_fusion
  32.5 18.5 %all-to-all-done = bf16[16,256,128]{1,2,0:T(8,128)(2,1)S(1)} async-done(((bf16[16,256,128]{1,2,0:T(8,128)(2,1)}), bf16[16,256,128]{1,2,0:T(8,128)(2,1)S(1)}, u32[]{:S(2)}, u32[]{:S(2)}) %all-to-all-start) | async-done | bytes 1048608 | tf_op jit(solution)/shard_map/all_to_all | solution.py:17
  51.0 1.8 multiply_reduce_fusion.1
  52.8 0.6 broadcast_in_dim.45
  53.5 6.8 %all-to-all-start.1 = ((f32[16,1,256]{2,1,0:T(1,128)}), f32[16,1,256]{2,1,0:T(1,128)S(1)}, u32[]{:S(2)}, u32[]{:S(2)}) async-start(f32[16,1,256]{2,1,0:T(1,128)} %broadcast_in_dim.45), calls=%async_computation.1 | async-start | bytes 32768 | tf_op jit(solution)/shard_map/all_to_all | solution.py:17
  60.3 0.0 all-gather.3.cloned.1.call-start
  60.3 0.7 convert_element_type.64
  61.0 5.5 %all-to-all-done.1 = f32[16,1,256]{2,1,0:T(1,128)S(1)} async-done(((f32[16,1,256]{2,1,0:T(1,128)}), f32[16,1,256]{2,1,0:T(1,128)S(1)}, u32[]{:S(2)}, u32[]{:S(2)}) %all-to-all-start.1) | async-done | bytes 16416 | tf_op jit(solution)/shard_map/all_to_all | solution.py:17
  66.6 0.1 multiply_convert_fusion
  66.7 3.9 %gather_fusion = bf16[1024,256]{1,0:T(8,128)(2,1)S(1)} fusion(bf16[257,256]{1,0:T(8,128)(2,1)S(1)} %concatenate.11, s32[1024]{0:T(1024)S(1)} %fusion.20), kind=kCustom, calls=%fused_computation | custom fusion | bytes 1052672 | tf_op jit(solution)/shard_map/gather | solution.py:91
  70.7 32.5 %all_to_all.21 = bf16[32,32,256]{2,1,0:T(8,128)(2,1)} all-to-all(bf16[32,32,256]{2,1,0:T(8,128)(2,1)S(1)} %bitcast.51), channel_id=1, replica_groups=mesh['sp'=32,'tp'=16] {'sp'}, dimensions={0} | all-to-all | bytes 1048576 | tf_op jit(solution)/shard_map/all_to_all | solution.py:92
  103.2 0.0 all-gather.3.cloned.1.call-update
  103.2 0.0 all-gather.5.cloned.1.call-start
  103.2 58.8 %all-gather.3.cloned.1.call-done = bf16[1024,4096]{1,0:T(8,128)(2,1)} async-done(((bf16[1024,256]{1,0:T(8,128)(2,1)}), bf16[1024,4096]{1,0:T(8,128)(2,1)}) %all-gather.3.cloned.1.call-update) | async-done | bytes 8388624 | tf_op jit(solution)/shard_map/all_gather | solution.py:95
  162.0 0.0 copy-done.4
  162.0 0.0 copy-start.3
  162.0 0.0 copy-start.5
  162.0 5.9 %fusion.5 = f32[1024,128]{1,0:T(8,128)S(1)} fusion(bf16[1024,4096]{1,0:T(8,128)(2,1)} %all-gather.3.cloned.1.call-done, bf16[1,4096,128]{2,1,0:T(8,128)(2,1)S(1)} %copy-done.4), kind=kOutput, calls=%fused_computation.11 | convolution fusion | flops 1073741824 | bytes 9961472 | tf_op jit(solution)/shard_map/dot_general | solution.py:96
  167.9 0.0 copy-done.3
  167.9 0.1 copy-done.5
  168.0 0.0 copy-start.1
  168.0 0.0 copy-start.2
  168.0 3.0 %fusion = bf16[1024,128]{1,0:T(8,128)(2,1)} fusion(bf16[1024,4096]{1,0:T(8,128)(2,1)S(1)} %copy-done.3, bf16[1,4096,128]{2,1,0:T(8,128)(2,1)S(1)} %copy-done.5, f32[1024,128]{1,0:T(8,128)S(1)} %fusion.5), kind=kOutput, calls=%fused_computation.5 | convolution fusion | flops 1074528256 | bytes 10223616 | tf_op jit(solution)/shard_map/dot_general | solution.py:97
  171.0 0.0 all-gather.5.cloned.1.call-update
  171.0 49.6 %all-gather.5.cloned.1.call-done = bf16[1024,2048]{1,0:T(8,128)(2,1)} async-done(((bf16[1024,128]{1,0:T(8,128)(2,1)}), bf16[1024,2048]{1,0:T(8,128)(2,1)}) %all-gather.5.cloned.1.call-update) | async-done | bytes 4194320 | tf_op jit(solution)/shard_map/all_gather | solution.py:101
  220.6 0.0 copy-done
  220.6 4.2 %convolution_convert_fusion = bf16[1024,256]{1,0:T(8,128)(2,1)} fusion(bf16[1024,2048]{1,0:T(8,128)(2,1)} %all-gather.5.cloned.1.call-done, bf16[1,2048,256]{2,1,0:T(8,128)(2,1)S(1)} %copy-done), kind=kOutput, calls=%fused_computation.3 | convolution fusion | flops 1074003968 | bytes 5767168 | tf_op jit(solution)/shard_map/dot_general | solution.py:100
  224.9 10.2 %all-to-all-start.3 = ((bf16[32,32,256]{2,1,0:T(8,128)(2,1)}), bf16[32,32,256]{2,1,0:T(8,128)(2,1)S(1)}, u32[]{:S(2)}, u32[]{:S(2)}) async-start(bf16[32,32,256]{2,1,0:T(8,128)(2,1)} %bitcast.13), calls=%async_computation.3 | async-start | bytes 1048576 | tf_op jit(solution)/shard_map/all_to_all | solution.py:105
  235.0 0.0 copy-done.1
  235.1 0.0 copy-done.2
  235.1 0.1 copy.34
  235.3 18.0 %all-to-all-done.3 = bf16[32,32,256]{2,1,0:T(8,128)(2,1)S(1)} async-done(((bf16[32,32,256]{2,1,0:T(8,128)(2,1)}), bf16[32,32,256]{2,1,0:T(8,128)(2,1)S(1)}, u32[]{:S(2)}, u32[]{:S(2)}) %all-to-all-start.3) | async-done | bytes 524320 | tf_op jit(solution)/shard_map/all_to_all | solution.py:105
  253.3 1.9 gather_fusion.1
  255.2 0.3 reshape.85
  255.5 0.7 multiply_reduce_fusion
  256.2 0.7 add_convert_fusion
  (14 shorter events, 0.2 us)
Async XLA Ops:
  6.5 214.1 %copy-start = (bf16[1,2048,256]{2,1,0:T(8,128)(2,1)S(1)}, bf16[1,2048,256]{2,1,0:T(8,128)(2,1)}, u32[]{:S(2)}) copy-start(bf16[1,2048,256]{2,1,0:T(8,128)(2,1)} %param.27) | copy-start | bytes 3145732
  6.5 155.5 %copy-start.4 = (bf16[1,4096,128]{2,1,0:T(8,128)(2,1)S(1)}, bf16[1,4096,128]{2,1,0:T(8,128)(2,1)}, u32[]{:S(2)}) copy-start(bf16[1,4096,128]{2,1,0:T(8,128)(2,1)} %param.25) | copy-start | bytes 3145732
  7.4 8.4 %collective-permute-start = (f32[2]{0:T(128)S(1)}, f32[2]{0:T(128)S(1)}, u32[]{:S(2)}, u32[]{:S(2)}) collective-permute-start(f32[2]{0:T(128)S(1)} %slice.34), channel_id=1, source_target_pairs={{0,16},{16,32},{32,48},{48,64},{64,80},{80,96},{96,112},{112,128},... | collective-permute-start | bytes 32 | tf_op jit(solution)/shard_map/ppermute | solution.py:12
  11.7 4.9 %collective-permute-start.1 = (f32[2,128]{1,0:T(2,128)S(1)}, f32[2,128]{1,0:T(2,128)S(1)}, u32[]{:S(2)}, u32[]{:S(2)}) collective-permute-start(f32[2,128]{1,0:T(2,128)S(1)} %slice.48), channel_id=1, source_target_pairs={{0,16},{16,32},{32,48},{48,64},{64,80},{80,96},{96,112},{112,128},... | collective-permute-start | bytes 3080 | tf_op jit(solution)/shard_map/ppermute | solution.py:12
  18.9 32.2 %all-to-all-start = ((bf16[16,256,128]{1,2,0:T(8,128)(2,1)}), bf16[16,256,128]{1,2,0:T(8,128)(2,1)S(1)}, u32[]{:S(2)}, u32[]{:S(2)}) async-start(bf16[16,256,128]{1,2,0:T(8,128)(2,1)} %broadcast_in_dim.44), calls=%async_computation | async-start | bytes 2097152 | tf_op jit(solution)/shard_map/all_to_all | solution.py:17
  53.5 13.1 %all-to-all-start.1 = ((f32[16,1,256]{2,1,0:T(1,128)}), f32[16,1,256]{2,1,0:T(1,128)S(1)}, u32[]{:S(2)}, u32[]{:S(2)}) async-start(f32[16,1,256]{2,1,0:T(1,128)} %broadcast_in_dim.45), calls=%async_computation.1 | async-start | bytes 32768 | tf_op jit(solution)/shard_map/all_to_all | solution.py:17
  60.3 101.7 %all-gather.3.cloned.1.call-start = ((), (), s32[]{:S(2)}) async-start(), calls=%async_computation.4 | async-start | bytes 8912896 | tf_op jit(solution)/shard_map/all_gather | solution.py:95
  103.2 117.4 %all-gather.5.cloned.1.call-start = ((), (), s32[]{:S(2)}) async-start(), calls=%async_computation.5 | async-start | bytes 4456448 | tf_op jit(solution)/shard_map/all_gather | solution.py:101
  162.0 5.9 %copy-start.3 = (bf16[1024,4096]{1,0:T(8,128)(2,1)S(1)}, bf16[1024,4096]{1,0:T(8,128)(2,1)}, u32[]{:S(2)}) copy-start(bf16[1024,4096]{1,0:T(8,128)(2,1)} %all-gather.3.cloned.1.call-done) | copy-start | bytes 25165828
  162.0 6.0 %copy-start.5 = (bf16[1,4096,128]{2,1,0:T(8,128)(2,1)S(1)}, bf16[1,4096,128]{2,1,0:T(8,128)(2,1)}, u32[]{:S(2)}) copy-start(bf16[1,4096,128]{2,1,0:T(8,128)(2,1)} %param.26) | copy-start | bytes 3145732
  168.0 67.1 %copy-start.1 = (f32[256,2]{0,1:T(2,128)S(1)}, f32[256,2]{0,1:T(2,128)}, u32[]{:S(2)}) copy-start(f32[256,2]{0,1:T(2,128)} %param.24) | copy-start | bytes 6148
  168.0 67.1 %copy-start.2 = (f32[256]{0:T(256)S(1)}, f32[256]{0:T(256)}, u32[]{:S(2)}) copy-start(f32[256]{0:T(256)} %param.23) | copy-start | bytes 3076
  224.9 28.4 %all-to-all-start.3 = ((bf16[32,32,256]{2,1,0:T(8,128)(2,1)}), bf16[32,32,256]{2,1,0:T(8,128)(2,1)S(1)}, u32[]{:S(2)}, u32[]{:S(2)}) async-start(bf16[32,32,256]{2,1,0:T(8,128)(2,1)} %bitcast.13), calls=%async_computation.3 | async-start | bytes 1048576 | tf_op jit(solution)/shard_map/all_to_all | solution.py:105
Sparse Core Ops, SparseCore 0:
  103.3 58.6 all-gather.2
  171.2 49.4 all-gather.4
where the time goes:
time: 264 us
  waiting for transfers between devices  150 us (57%)
  blocking collectives  32.5 us (12%)
  starting transfers between devices  31.4 us (12%)
  matrix products  14.9 us (6%)
  between operations  13.6 us (5%)
  local copies, waits for them, and re-layouts  12.4 us (5%)
  other arithmetic  8.46 us (3%)
    all_gather x1, waiting for transfers between devices, per_device(): piece = lax.all_gather(arrived, 'tp', axis=1, tiled=True)  58.8 us
    all_gather x1, waiting for transfers between devices, per_device(): lax.all_gather(hidden, 'tp', axis=1, tiled=True)  49.6 us
    all_to_all x1, blocking collectives, per_device(): lax.all_to_all(outgoing, 'sp', split_axis=0, concat_axis=0, tiled=True)  32.5 us
    all_to_all x2, waiting for transfers between devices, from_everyone(): return lax.all_to_all(copies, axis, split_axis=0, concat_axis=0, tiled=True)  24 us
    all_to_all x1, waiting for transfers between devices, per_device(): lax.all_to_all(expert_out.reshape(experts, capacity, cols_local), 'sp', s...  18 us
    all_to_all x2, starting transfers between devices, from_everyone(): return lax.all_to_all(copies, axis, split_axis=0, concat_axis=0, tiled=True)  14.4 us
    all_to_all x1, starting transfers between devices, per_device(): lax.all_to_all(expert_out.reshape(experts, capacity, cols_local), 'sp', s...  10.2 us
    ppermute x2, starting transfers between devices, passed_along(): lax.ppermute(value, axis, [(source, source + steps) for source in range(i...  6.78 us
  transfers between devices with their start and end apart: 7, of which 5 were waited for; matrix products, arithmetic and copies ran while one was open for 4% of the time, Pallas kernels for 0%

commit v1 on v0

--- a/solution.py
+++ b/solution.py
@@ -2,6 +2,7 @@
 import jax.numpy as jnp
 from jax import lax
 from jax.sharding import PartitionSpec as P
+from jax.lax import all_to_all, axis_size
 
 EPS = 1e-06
 
@@ -97,10 +98,15 @@
     up_val = jnp.dot(piece, up_local, preferred_element_type=jnp.float32)
     hidden = (jax.nn.silu(gate_val) * up_val).astype(jnp.bfloat16)
     down_local = down_weight[0]
+
+    def play_the_teams(payload):
+        mesh_name = "tp"
+        row_out = jnp.concatenate(axis_size(mesh_name) * [payload], 1)
+        ready = all_to_all(row_out, mesh_name, 1, 1, tiled=True)
+        return ready
+
     expert_out = jnp.dot(
-        lax.all_gather(hidden, "tp", axis=1, tiled=True),
-        down_local,
-        preferred_element_type=jnp.float32,
+        play_the_teams(hidden), down_local, preferred_element_type=jnp.float32
     ).astype(jnp.bfloat16)
     returned = lax.all_to_all(
         expert_out.reshape(experts, capacity, cols_local),

time: 264 us -> 313 us (1.19)
  the two profiles are of different devices: /device:TPU:8 before, /device:TPU:1 now
where the time goes in v1:
time: 313 us
  blocking collectives  131 us (42%)
  waiting for transfers between devices  109 us (35%)
  starting transfers between devices  26 us (8%)
  between operations  13.8 us (4%)
  matrix products  13.3 us (4%)
  local copies, waits for them, and re-layouts  12.6 us (4%)
  other arithmetic  7.06 us (2%)
    all_to_all x1, blocking collectives, play_the_teams(): ready = all_to_all(row_out, mesh_name, 1, 1, tiled=True)  100 us
    all_gather x1, waiting for transfers between devices, per_device(): piece = lax.all_gather(arrived, 'tp', axis=1, tiled=True)  62.4 us
    all_to_all x1, blocking collectives, per_device(): lax.all_to_all(outgoing, 'sp', split_axis=0, concat_axis=0, tiled=True)  30.8 us
    all_to_all x2, waiting for transfers between devices, from_everyone(): return lax.all_to_all(copies, axis, split_axis=0, concat_axis=0, tiled=True)  29.8 us
    all_to_all x1, waiting for transfers between devices, per_device(): lax.all_to_all(expert_out.reshape(experts, capacity, cols_local), 'sp', s...  16.8 us
    all_to_all x2, starting transfers between devices, from_everyone(): return lax.all_to_all(copies, axis, split_axis=0, concat_axis=0, tiled=True)  11.8 us
    all_to_all x1, starting transfers between devices, per_device(): lax.all_to_all(expert_out.reshape(experts, capacity, cols_local), 'sp', s...  7.14 us
    ppermute x2, starting transfers between devices, passed_along(): lax.ppermute(value, axis, [(source, source + steps) for source in range(i...  7.04 us
  transfers between devices with their start and end apart: 6, of which 4 were waited for; matrix products, arithmetic and copies ran while one was open for 3% of the time, Pallas kernels for 0%

profile of v1, /device:TPU:1, one launch (start us, length us, event | category | flops | bytes accessed | tf_op | source)
XLA Modules:
  0.0 312.5 jit_solution(3647369513853047622)
XLA Ops:
  6.5 0.0 copy-start
  6.5 0.0 copy-start.4
  6.5 0.0 copy-start.3
  6.5 0.0 copy-start.8
  6.5 0.8 convert_element_type.60
  7.3 0.1 slice.34
  7.4 3.9 %collective-permute-start = (f32[2]{0:T(128)S(1)}, f32[2]{0:T(128)S(1)}, u32[]{:S(2)}, u32[]{:S(2)}) collective-permute-start(f32[2]{0:T(128)S(1)} %slice.34), channel_id=1, source_target_pairs={{0,16},{16,32},{32,48},{48,64},{64,80},{80,96},{96,112},{112,128},... | collective-permute-start | bytes 32 | tf_op jit(solution)/shard_map/ppermute | solution.py:13
  11.3 0.9 convert_multiply_fusion
  12.2 3.1 collective-permute-start.1
  15.4 0.7 convert_element_type.57
  16.0 0.0 collective-permute-done
  16.0 0.1 pad_maximum_fusion.1
  16.1 0.8 slice_compare_fusion.1
  16.9 0.0 collective-permute-done.1
  16.9 1.0 fusion.13
  17.9 0.1 copy.28
  18.0 1.1 broadcast_in_dim.44
  19.1 8.3 %all-to-all-start = ((bf16[16,256,128]{1,2,0:T(8,128)(2,1)}), bf16[16,256,128]{1,2,0:T(8,128)(2,1)S(1)}, u32[]{:S(2)}, u32[]{:S(2)}) async-start(bf16[16,256,128]{1,2,0:T(8,128)(2,1)} %broadcast_in_dim.44), calls=%async_computation | async-start | bytes 2097152 | tf_op jit(solution)/shard_map/all_to_all | solution.py:18
  27.4 0.8 copy.31
  28.2 0.1 eq.37
  28.4 0.1 eq.33
  28.5 1.2 reduce-window.6
  29.7 0.2 slice_reduce_fusion
  30.0 0.0 copy-done.4
  30.0 0.1 copy.30
  30.1 0.1 mul.115
  30.3 0.1 fusion.18
  30.4 2.4 scatter_custom_fusion
  32.9 22.6 %all-to-all-done = bf16[16,256,128]{1,2,0:T(8,128)(2,1)S(1)} async-done(((bf16[16,256,128]{1,2,0:T(8,128)(2,1)}), bf16[16,256,128]{1,2,0:T(8,128)(2,1)S(1)}, u32[]{:S(2)}, u32[]{:S(2)}) %all-to-all-start) | async-done | bytes 1048608 | tf_op jit(solution)/shard_map/all_to_all | solution.py:18
  55.4 0.0 copy-done.3
  55.4 0.0 copy-start.2
  55.4 1.9 multiply_reduce_fusion.1
  57.3 0.6 broadcast_in_dim.45
  57.9 3.4 %all-to-all-start.1 = ((f32[16,1,256]{2,1,0:T(1,128)}), f32[16,1,256]{2,1,0:T(1,128)S(1)}, u32[]{:S(2)}, u32[]{:S(2)}) async-start(f32[16,1,256]{2,1,0:T(1,128)} %broadcast_in_dim.45), calls=%async_computation.1 | async-start | bytes 32768 | tf_op jit(solution)/shard_map/all_to_all | solution.py:18
  61.3 0.0 all-gather.2.cloned.1.call-start
  61.4 0.0 copy-done.8
  61.4 7.3 %all-to-all-done.1 = f32[16,1,256]{2,1,0:T(1,128)S(1)} async-done(((f32[16,1,256]{2,1,0:T(1,128)}), f32[16,1,256]{2,1,0:T(1,128)S(1)}, u32[]{:S(2)}, u32[]{:S(2)}) %all-to-all-start.1) | async-done | bytes 16416 | tf_op jit(solution)/shard_map/all_to_all | solution.py:18
  68.7 0.1 multiply_convert_fusion
  68.9 3.9 %gather_fusion = bf16[1024,256]{1,0:T(8,128)(2,1)S(1)} fusion(bf16[257,256]{1,0:T(8,128)(2,1)S(1)} %concatenate.14, s32[1024]{0:T(1024)S(1)} %fusion.20), kind=kCustom, calls=%fused_computation | custom fusion | bytes 1052672 | tf_op jit(solution)/shard_map/gather | solution.py:92
  72.8 30.8 %all_to_all.33 = bf16[32,32,256]{2,1,0:T(8,128)(2,1)} all-to-all(bf16[32,32,256]{2,1,0:T(8,128)(2,1)S(1)} %bitcast.57), channel_id=1, replica_groups=mesh['sp'=32,'tp'=16] {'sp'}, dimensions={0} | all-to-all | bytes 1048576 | tf_op jit(solution)/shard_map/all_to_all | solution.py:93
  103.6 0.0 all-gather.2.cloned.1.call-update
  103.6 62.4 %all-gather.2.cloned.1.call-done = bf16[1024,4096]{1,0:T(8,128)(2,1)} async-done(((bf16[1024,256]{1,0:T(8,128)(2,1)}), bf16[1024,4096]{1,0:T(8,128)(2,1)}) %all-gather.2.cloned.1.call-update) | async-done | bytes 8388624 | tf_op jit(solution)/shard_map/all_gather | solution.py:96
  166.0 0.0 copy-done.2
  166.0 0.0 copy-start.1
  166.0 6.4 %fusion.5 = f32[1024,128]{0,1:T(8,128)S(1)} fusion(bf16[1024,4096]{1,0:T(8,128)(2,1)} %all-gather.2.cloned.1.call-done, bf16[1,4096,128]{2,1,0:T(8,128)(2,1)S(1)} %copy-done.2), kind=kOutput, calls=%fused_computation.11 | convolution fusion | flops 1073741824 | bytes 9961472 | tf_op jit(solution)/shard_map/dot_general | solution.py:97
  172.5 0.0 copy-done
  172.5 0.0 copy-done.1
  172.5 2.9 constant_dynamic-update-slice_fusion.15
  175.8 0.0 copy-start.7
  175.8 100.0 %all_to_all.34 = bf16[1024,16,128]{0,2,1:T(8,128)(2,1)S(1)} all-to-all(bf16[1024,16,128]{0,2,1:T(8,128)(2,1)S(1)} %bitcast.53), channel_id=1, replica_groups=mesh['sp'=32,'tp'=16] {'tp'}, dimensions={1} | all-to-all | bytes 8388608 | tf_op jit(solution)/shard_map/all_to_all | solution.py:105
  275.8 0.0 copy-done.7
  275.8 0.0 copy-start.5
  275.8 0.0 copy-start.6
  275.8 2.1 convolution_convert_fusion
  277.9 7.1 %all-to-all-start.4 = ((bf16[32,32,256]{2,1,0:T(8,128)(2,1)}), bf16[32,32,256]{2,1,0:T(8,128)(2,1)S(1)}, u32[]{:S(2)}, u32[]{:S(2)}) async-start(bf16[32,32,256]{2,1,0:T(8,128)(2,1)} %bitcast.15), calls=%async_computation.4 | async-start | bytes 1048576 | tf_op jit(solution)/shard_map/all_to_all | solution.py:111
  285.1 0.0 copy-done.5
  285.1 0.0 copy-done.6
  285.1 0.1 copy.34
  285.3 16.8 %all-to-all-done.4 = bf16[32,32,256]{2,1,0:T(8,128)(2,1)S(1)} async-done(((bf16[32,32,256]{2,1,0:T(8,128)(2,1)}), bf16[32,32,256]{2,1,0:T(8,128)(2,1)S(1)}, u32[]{:S(2)}, u32[]{:S(2)}) %all-to-all-start.4) | async-done | bytes 524320 | tf_op jit(solution)/shard_map/all_to_all | solution.py:111
  302.1 1.9 gather_fusion.1
  304.0 0.3 reshape.87
  304.3 0.7 multiply_reduce_fusion
  305.0 0.7 add_convert_fusion
  (31 shorter events, 0.5 us)
Async XLA Ops:
  6.5 165.9 %copy-start = (bf16[1,4096,128]{2,1,0:T(8,128)(2,1)S(1)}, bf16[1,4096,128]{2,1,0:T(8,128)(2,1)}, u32[]{:S(2)}) copy-start(bf16[1,4096,128]{2,1,0:T(8,128)(2,1)} %param.26) | copy-start | bytes 3145732
  6.5 23.4 %copy-start.4 = (s32[256,2]{0,1:T(2,128)S(1)}, s32[256,2]{0,1:T(2,128)}, u32[]{:S(2)}) copy-start(s32[256,2]{0,1:T(2,128)} %param.22) | copy-start | bytes 6148
  6.5 48.9 %copy-start.3 = (bf16[256,256]{1,0:T(8,128)(2,1)S(1)}, bf16[256,256]{1,0:T(8,128)(2,1)}, u32[]{:S(2)}) copy-start(bf16[256,256]{1,0:T(8,128)(2,1)} %param.20) | copy-start | bytes 393220
  6.5 54.9 %copy-start.8 = (bf16[256]{0:T(256)(128)(2,1)S(1)}, bf16[256]{0:T(256)(128)(2,1)}, u32[]{:S(2)}) copy-start(bf16[256]{0:T(256)(128)(2,1)} %param.21) | copy-start | bytes 1540
  7.4 8.7 %collective-permute-start = (f32[2]{0:T(128)S(1)}, f32[2]{0:T(128)S(1)}, u32[]{:S(2)}, u32[]{:S(2)}) collective-permute-start(f32[2]{0:T(128)S(1)} %slice.34), channel_id=1, source_target_pairs={{0,16},{16,32},{32,48},{48,64},{64,80},{80,96},{96,112},{112,128},... | collective-permute-start | bytes 32 | tf_op jit(solution)/shard_map/ppermute | solution.py:13
  12.2 4.7 %collective-permute-start.1 = (f32[2,128]{1,0:T(2,128)S(1)}, f32[2,128]{1,0:T(2,128)S(1)}, u32[]{:S(2)}, u32[]{:S(2)}) collective-permute-start(f32[2,128]{1,0:T(2,128)S(1)} %slice.48), channel_id=1, source_target_pairs={{0,16},{16,32},{32,48},{48,64},{64,80},{80,96},{96,112},{112,128},... | collective-permute-start | bytes 3080 | tf_op jit(solution)/shard_map/ppermute | solution.py:13
  19.1 36.3 %all-to-all-start = ((bf16[16,256,128]{1,2,0:T(8,128)(2,1)}), bf16[16,256,128]{1,2,0:T(8,128)(2,1)S(1)}, u32[]{:S(2)}, u32[]{:S(2)}) async-start(bf16[16,256,128]{1,2,0:T(8,128)(2,1)} %broadcast_in_dim.44), calls=%async_computation | async-start | bytes 2097152 | tf_op jit(solution)/shard_map/all_to_all | solution.py:18
  55.4 110.6 %copy-start.2 = (bf16[1,4096,128]{2,1,0:T(8,128)(2,1)S(1)}, bf16[1,4096,128]{2,1,0:T(8,128)(2,1)}, u32[]{:S(2)}) copy-start(bf16[1,4096,128]{2,1,0:T(8,128)(2,1)} %param.25) | copy-start | bytes 3145732
  57.9 10.8 %all-to-all-start.1 = ((f32[16,1,256]{2,1,0:T(1,128)}), f32[16,1,256]{2,1,0:T(1,128)S(1)}, u32[]{:S(2)}, u32[]{:S(2)}) async-start(f32[16,1,256]{2,1,0:T(1,128)} %broadcast_in_dim.45), calls=%async_computation.1 | async-start | bytes 32768 | tf_op jit(solution)/shard_map/all_to_all | solution.py:18
  61.3 104.7 %all-gather.2.cloned.1.call-start = ((), (), s32[]{:S(2)}) async-start(), calls=%async_computation.5 | async-start | bytes 8912896 | tf_op jit(solution)/shard_map/all_gather | solution.py:96
  166.0 6.4 %copy-start.1 = (bf16[1024,4096]{1,0:T(8,128)(2,1)S(1)}, bf16[1024,4096]{1,0:T(8,128)(2,1)}, u32[]{:S(2)}) copy-start(bf16[1024,4096]{1,0:T(8,128)(2,1)} %all-gather.2.cloned.1.call-done) | copy-start | bytes 25165828
  175.8 100.0 %copy-start.7 = (bf16[1,2048,256]{2,1,0:T(8,128)(2,1)S(1)}, bf16[1,2048,256]{2,1,0:T(8,128)(2,1)}, u32[]{:S(2)}) copy-start(bf16[1,2048,256]{2,1,0:T(8,128)(2,1)} %param.27) | copy-start | bytes 3145732
  275.8 9.3 %copy-start.5 = (f32[256,2]{0,1:T(2,128)S(1)}, f32[256,2]{0,1:T(2,128)}, u32[]{:S(2)}) copy-start(f32[256,2]{0,1:T(2,128)} %param.24) | copy-start | bytes 6148
  275.8 9.3 %copy-start.6 = (f32[256]{0:T(256)S(1)}, f32[256]{0:T(256)}, u32[]{:S(2)}) copy-start(f32[256]{0:T(256)} %param.23) | copy-start | bytes 3076
  277.9 24.1 %all-to-all-start.4 = ((bf16[32,32,256]{2,1,0:T(8,128)(2,1)}), bf16[32,32,256]{2,1,0:T(8,128)(2,1)S(1)}, u32[]{:S(2)}, u32[]{:S(2)}) async-start(bf16[32,32,256]{2,1,0:T(8,128)(2,1)} %bitcast.15), calls=%async_computation.4 | async-start | bytes 1048576 | tf_op jit(solution)/shard_map/all_to_all | solution.py:111
Sparse Core Ops, SparseCore 0:
  103.7 62.2 all-gather.1
